TPU v7x, 32 devices: a whole 2x2x4 slice. The times are simulated.
32 devices in a mesh: grp: 2 (over y), sp: 4 (over z), tp: 4 (over x, core).
Axes of the slice: x: 2, y: 2, z: 4, core: 2. Of those that a mesh axis runs over, the one named last changes fastest.
Arguments:
- hidden_in: bfloat16 [3072, 4096], P(('grp', 'sp'), 'tp'), parts along dimension 0, may hold values from -30 to 30
- in_gain: float32 [2, 4096], P(None, 'tp'), may hold values from 0.1 to 1.9
- w_value: bfloat16 [2, 4096, 2048], P(None, 'sp', 'tp'), may hold values from -0.09375 to 0.09375
- w_gate: bfloat16 [2, 4096, 2048], P(None, 'sp', 'tp'), may hold values from -0.09375 to 0.09375
- conv_taps: float32 [2, 31, 2048], P(None, None, 'tp'), may hold values from -9 to 9
- norm_gain: float32 [2, 2048], P(None, 'tp'), may hold values from 0.1 to 1.9
- norm_shift: float32 [2, 2048], P(None, 'tp'), may hold values from -3 to 3
- w_out: bfloat16 [2, 2048, 4096], P(None, 'tp', 'sp'), may hold values from -0.125 to 0.125
Outputs:
- hidden_out: bfloat16 [3072, 4096], P(('grp', 'sp'), 'tp'), parts along dimension 0
There are 2 independent parts, one for each index of `grp`. A program takes and returns all parts, laid end to end along the dimension named above; an argument that names none is the same for every part. Nothing has to cross between parts.
All inputs are finite; a program needn't handle non-finite values.
Results may differ from a plain program's by a relative error of at most 0.013.
Values may be sent and summed in bfloat16 or wider, within the bound.
A program may use at most 64 MiB of HBM per device.

v0:
```python
import jax
import jax.numpy as jnp
from jax import lax
from jax.sharding import PartitionSpec as P

D = 4096
C = 2048
epsilon = 1e-06


def passed_along(value, axis, steps):
    count = lax.axis_size(axis)
    initial, last = (max(0, -steps), min(count, count - steps))
    return lax.ppermute(value, axis, [(source, source + steps) for source in range(initial, last)])


def depthwise(extended, kernel_taps):
    conved = lax.conv_general_dilated(
        extended.astype(jnp.float32)[None],
        kernel_taps[:, None, :],
        (1,),
        [(0, 0)],
        dimension_numbers=("NWC", "WIO", "NWC"),
        feature_group_count=extended.shape[1],
        precision=lax.Precision.HIGHEST,
    )
    return conved[0]


def shards(hidden_in, in_gain, w_value, w_gate, conv_taps, norm_gain, norm_shift, w_out):
    layer_count = w_value.shape[0]
    reach_rows = conv_taps.shape[1] - 1
    value_all, gate_all = (
        lax.all_gather(w_value, "sp", axis=1, tiled=True),
        lax.all_gather(w_gate, "sp", axis=1, tiled=True),
    )
    out_all = lax.all_gather(w_out, "sp", axis=2, tiled=True)
    current = hidden_in
    for layer_idx in range(layer_count):
        widened = current.astype(jnp.float32)
        squares = lax.psum(jnp.sum(widened * widened, axis=1), "tp")
        normalized = (
            widened * lax.rsqrt(squares / D + epsilon)[:, None] * in_gain[layer_idx]
        ).astype(jnp.bfloat16)
        gathered = lax.all_gather(normalized, "tp", axis=1, tiled=True)
        value_part = jnp.dot(gathered, value_all[layer_idx], preferred_element_type=jnp.float32)
        gate_part = jnp.dot(gathered, gate_all[layer_idx], preferred_element_type=jnp.float32)
        gated = (value_part * jax.nn.sigmoid(gate_part)).astype(jnp.bfloat16)
        before = passed_along(gated[gated.shape[0] - reach_rows :], "sp", 1)
        extended = jnp.concatenate([before, gated], axis=0)
        residual = current
        conved = depthwise(extended, conv_taps[layer_idx])
        total_sum, total_squares = lax.psum(
            (jnp.sum(conved, axis=1), jnp.sum(conved * conved, axis=1)), "tp"
        )
        row_mean = total_sum / C
        spread = total_squares / C - row_mean * row_mean
        normed = (conved - row_mean[:, None]) * lax.rsqrt(spread + epsilon)[:, None] * norm_gain[
            layer_idx
        ] + norm_shift[layer_idx]
        mixed_out = jax.nn.silu(normed).astype(jnp.bfloat16)
        partial_value = jnp.dot(mixed_out, out_all[layer_idx], preferred_element_type=jnp.float32)
        summed = lax.psum_scatter(
            partial_value.astype(jnp.bfloat16), "tp", scatter_dimension=1, tiled=True
        ).astype(jnp.float32)
        current = (residual.astype(jnp.float32) + summed).astype(jnp.bfloat16)
    return current


def solution(mesh):
    placed = (
        P(("grp", "sp"), "tp"),
        P(None, "tp"),
        P(None, "sp", "tp"),
        P(None, "sp", "tp"),
        P(None, None, "tp"),
        P(None, "tp"),
        P(None, "tp"),
        P(None, "tp", "sp"),
    )
    return jax.shard_map(
        shards, mesh=mesh, in_specs=placed, out_specs=P(("grp", "sp"), "tp"), check_vma=False
    )
```

profile of v0, /device:TPU:0, one launch (start us, length us, event | category | flops | bytes accessed | tf_op | source)
XLA Modules:
  0.0 657.1 jit_solution(9422213232833642842)
XLA Ops:
  7.9 8.4 %psum.42 = f32[384]{0:T(512)S(1)} all-reduce(f32[384]{0:T(512)S(1)} %fusion.4), channel_id=1, replica_groups=mesh['grp'=2,'sp'=4,'tp'=4] {'tp'}, use_global_device_ids=true, to_apply=%region_1.0 | all-reduce | flops 384 | bytes 3072 | tf_op jit(solution)/shard_map/psum | solution.py:41
  17.1 2.3 fusion.6
  21.5 26.8 %all-gather.6.cloned.1.call-done = bf16[384,4096]{1,0:T(8,128)(2,1)} async-done(((bf16[384,1024]{1,0:T(8,128)(2,1)}), bf16[384,4096]{1,0:T(8,128)(2,1)}) %all-gather.6.cloned.1.call-update) | async-done | bytes 3145744 | tf_op jit(solution)/shard_map/all_gather | solution.py:45
  48.3 151.2 %all-gather.10.cloned.1.call-done = bf16[2,4096,512]{2,1,0:T(8,128)(2,1)} async-done(((bf16[2,1024,512]{2,1,0:T(8,128)(2,1)}), bf16[2,4096,512]{2,1,0:T(8,128)(2,1)}) %all-gather.10.cloned.1.call-update) | async-done | bytes 8388624 | tf_op jit(solution)/shard_map/all_gather | solution.py:35
  199.5 5.9 fusion.23
  205.5 143.5 %all-gather.8.cloned.1.call-done = bf16[2,4096,512]{2,1,0:T(8,128)(2,1)} async-done(((bf16[2,1024,512]{2,1,0:T(8,128)(2,1)}), bf16[2,4096,512]{2,1,0:T(8,128)(2,1)}) %all-gather.8.cloned.1.call-update) | async-done | bytes 8388624 | tf_op jit(solution)/shard_map/all_gather | solution.py:34
  349.0 4.2 fusion.25
  356.6 1.9 fusion.65
  359.9 6.6 all-reduce.1
  366.5 131.7 %all-gather.12.cloned.1.call-done = bf16[2,512,4096]{2,1,0:T(8,128)(2,1)} async-done(((bf16[2,512,1024]{2,1,0:T(8,128)(2,1)}), bf16[2,512,4096]{2,1,0:T(8,128)(2,1)}) %all-gather.12.cloned.1.call-update) | async-done | bytes 8388624 | tf_op jit(solution)/shard_map/all_gather | solution.py:37
  498.2 5.9 convolution_convert_fusion.1
  504.2 36.0 %reduce-scatter.3.cloned.1.call-done = bf16[384,1024]{1,0:T(8,128)(2,1)} async-done(((bf16[384,4096]{1,0:T(8,128)(2,1)}), bf16[384,1024]{1,0:T(8,128)(2,1)}) %reduce-scatter.3.cloned.1.call-update) | async-done | bytes 786448 | tf_op jit(solution)/shard_map/reduce_scatter | solution.py:63
  541.6 5.8 psum.45
  547.4 2.3 fusion.10
  550.0 29.1 %all-gather.14.cloned.1.call-done = bf16[384,4096]{1,0:T(8,128)(2,1)} async-done(((bf16[384,1024]{1,0:T(8,128)(2,1)}), bf16[384,4096]{1,0:T(8,128)(2,1)}) %all-gather.14.cloned.1.call-update) | async-done | bytes 3145744 | tf_op jit(solution)/shard_map/all_gather | solution.py:45
  579.0 5.2 fusion.21
  584.2 4.0 fusion.24
  588.3 3.4 collective-permute-start.1
  591.7 1.6 collective-permute-done.1
  593.7 2.0 fusion.66
  597.2 5.9 all-reduce
  603.2 5.9 convolution_convert_fusion
  609.1 38.7 %reduce-scatter.5.cloned.1.call-done = bf16[384,1024]{1,0:T(8,128)(2,1)} async-done(((bf16[384,4096]{1,0:T(8,128)(2,1)}), bf16[384,1024]{1,0:T(8,128)(2,1)}) %reduce-scatter.5.cloned.1.call-update) | async-done | bytes 786448 | tf_op jit(solution)/shard_map/reduce_scatter | solution.py:63
  647.8 2.4 fusion.11
  (64 shorter events, 12.7 us)
Async XLA Ops:
  6.5 41.8 %all-gather.6.cloned.1.call-start = ((), (), s32[]{:S(2)}) async-start(), calls=%async_computation.2 | async-start | bytes 3932160 | tf_op jit(solution)/shard_map/all_gather | solution.py:45
  19.4 2.1 copy-start.2
  19.4 180.2 %all-gather.10.cloned.1.call-start = ((), (), s32[]{:S(2)}) async-start(), calls=%async_computation.4 | async-start | bytes 10485760 | tf_op jit(solution)/shard_map/all_gather | solution.py:35
  20.1 328.8 %all-gather.8.cloned.1.call-start = ((), (), s32[]{:S(2)}) async-start(), calls=%async_computation.3 | async-start | bytes 10485760 | tf_op jit(solution)/shard_map/all_gather | solution.py:34
  20.9 477.4 %all-gather.12.cloned.1.call-start = ((), (), s32[]{:S(2)}) async-start(), calls=%async_computation.5 | async-start | bytes 10485760 | tf_op jit(solution)/shard_map/all_gather | solution.py:37
  21.4 518.8 %reduce-scatter.3.cloned.1.call-start = ((), (), s32[]{:S(2)}) async-start(), calls=%async_computation.6 | async-start | bytes 3932160 | tf_op jit(solution)/shard_map/reduce_scatter | solution.py:63
  48.3 300.6 %copy-start.4 = (bf16[384,4096]{1,0:T(8,128)(2,1)S(1)}, bf16[384,4096]{1,0:T(8,128)(2,1)}, u32[]{:S(2)}) copy-start(bf16[384,4096]{1,0:T(8,128)(2,1)} %all-gather.6.cloned.1.call-done) | copy-start | bytes 9437188
  205.5 149.1 %copy-start.3 = (f32[2,512]{1,0:T(2,128)S(1)}, f32[2,512]{1,0:T(2,128)}, u32[]{:S(2)}) copy-start(f32[2,512]{1,0:T(2,128)} %param.14) | copy-start | bytes 12292
  353.1 3.5 copy-start.6
  353.2 3.5 copy-start.7
  353.2 3.0 collective-permute-start
  504.1 36.1 %copy-start = (bf16[384,1024]{1,0:T(8,128)(2,1)S(1)}, bf16[384,1024]{1,0:T(8,128)(2,1)}, u32[]{:S(2)}) copy-start(bf16[384,1024]{1,0:T(8,128)(2,1)} %param.8) | copy-start | bytes 2359300
  504.1 74.9 %all-gather.14.cloned.1.call-start = ((), (), s32[]{:S(2)}) async-start(), calls=%async_computation.7 | async-start | bytes 3932160 | tf_op jit(solution)/shard_map/all_gather | solution.py:45
  549.8 98.0 %reduce-scatter.5.cloned.1.call-start = ((), (), s32[]{:S(2)}) async-start(), calls=%async_computation.8 | async-start | bytes 3932160 | tf_op jit(solution)/shard_map/reduce_scatter | solution.py:63
  579.0 5.2 copy-start.5
  588.3 5.0 collective-permute-start.1
  609.1 38.7 %copy-start.1 = (bf16[384,1024]{1,0:T(8,128)(2,1)S(1)}, bf16[384,1024]{1,0:T(8,128)(2,1)}, u32[]{:S(2)}) copy-start(bf16[384,1024]{1,0:T(8,128)(2,1)} %reduce-scatter.3.cloned.1.call-done) | copy-start | bytes 2359300
Sparse Core Ops, SparseCore 0:
  19.5 28.8 all-gather.5
  49.9 149.6 all-gather.9
  201.1 147.7 all-gather.7
  350.4 147.7 all-gather.11
  504.2 35.8 reduce-scatter.2
  549.9 29.1 all-gather.13
  609.2 38.5 reduce-scatter.4
where the time goes:
time: 658 us; the launch traced here: 657 us
  waiting for transfers between devices  562 us (85%)
  matrix products  35 us (5%)
  blocking collectives  26.6 us (4%)
  between operations  13.8 us (2%)
  other arithmetic  10.6 us (2%)
    all_gather x1, waiting for transfers between devices, shards(): lax.all_gather(w_gate, 'sp', axis=1, tiled=True)  151 us
    all_gather x1, waiting for transfers between devices, shards(): lax.all_gather(w_value, 'sp', axis=1, tiled=True)  143 us
    all_gather x1, waiting for transfers between devices, shards(): out_all = lax.all_gather(w_out, 'sp', axis=2, tiled=True)  132 us
    reduce_scatter x2, waiting for transfers between devices, shards(): lax.psum_scatter(partial_value.astype(jnp.bfloat16), 'tp', scatter_dimens...  74.7 us
    all_gather x2, waiting for transfers between devices, shards(): gathered = lax.all_gather(normalized, 'tp', axis=1, tiled=True)  55.9 us
    psum x2, blocking collectives, shards(): squares = lax.psum(jnp.sum(widened * widened, axis=1), 'tp')  14.1 us
  transfers between devices with their start and end apart: 9, of which 9 were waited for; matrix products, arithmetic and copies ran while one was open for 2% of the time, Pallas kernels for 0%

commit v1 on v0

--- a/solution.py
+++ b/solution.py
@@ -34,7 +34,11 @@
         lax.all_gather(w_value, "sp", axis=1, tiled=True),
         lax.all_gather(w_gate, "sp", axis=1, tiled=True),
     )
-    out_all = lax.all_gather(w_out, "sp", axis=2, tiled=True)
+
+    def local_data_touch(buf):
+        return jnp.concatenate(lax.all_gather(buf, axis_name="sp"), 2)
+
+    out_all = local_data_touch(w_out)
     current = hidden_in
     for layer_idx in range(layer_count):
         widened = current.astype(jnp.float32)

time: 658 us -> 684 us (1.040)
  local copies, waits for them, and re-layouts: 3.79 us -> 22.6 us
  waiting for transfers between devices: 562 us -> 569 us
    slice x0 -> x3, local copies, waits for them, and re-layouts: none -> 18.3 us  [shards(): out_all[layer_idx]]
    all_gather x1, waiting for transfers between devices: 132 us -> 143 us  [local_data_touch(): return jnp.concatenate(lax.all_gather(buf, axis_name='sp'), 2)]
  transfers between devices with their start and end apart: 9 -> 9, of which waited for: 9 -> 7; matrix products, arithmetic and copies ran while one was open for 2% -> 4% of each run, Pallas kernels for 0% -> 0%
where the time goes in v1:
time: 684 us; the launch traced here: 683 us
  waiting for transfers between devices  569 us (83%)
  matrix products  34.8 us (5%)
  blocking collectives  26.9 us (4%)
  local copies, waits for them, and re-layouts  22.6 us (3%)
  between operations  13.8 us (2%)
  other arithmetic  10.6 us (2%)
    all_gather x1, waiting for transfers between devices, shards(): lax.all_gather(w_gate, 'sp', axis=1, tiled=True)  151 us
    all_gather x1, waiting for transfers between devices, shards(): lax.all_gather(w_value, 'sp', axis=1, tiled=True)  144 us
    all_gather x1, waiting for transfers between devices, local_data_touch(): return jnp.concatenate(lax.all_gather(buf, axis_name='sp'), 2)  143 us
    reduce_scatter x2, waiting for transfers between devices, shards(): lax.psum_scatter(partial_value.astype(jnp.bfloat16), 'tp', scatter_dimens...  73 us
    all_gather x2, waiting for transfers between devices, shards(): gathered = lax.all_gather(normalized, 'tp', axis=1, tiled=True)  55.9 us
    slice x3, local copies, waits for them, and re-layouts, shards(): out_all[layer_idx]  18.3 us
    psum x2, blocking collectives, shards(): squares = lax.psum(jnp.sum(widened * widened, axis=1), 'tp')  14.1 us
  transfers between devices with their start and end apart: 9, of which 7 were waited for; matrix products, arithmetic and copies ran while one was open for 4% of the time, Pallas kernels for 0%

profile of v1, /device:TPU:0, one launch (start us, length us, event | category | flops | bytes accessed | tf_op | source)
XLA Modules:
  0.0 683.0 jit_solution(12178636627643781210)
XLA Ops:
  8.7 8.4 %psum.42 = f32[384]{0:T(512)S(1)} all-reduce(f32[384]{0:T(512)S(1)} %fusion.4), channel_id=1, replica_groups=mesh['grp'=2,'sp'=4,'tp'=4] {'tp'}, use_global_device_ids=true, to_apply=%region_1.0 | all-reduce | flops 384 | bytes 3072 | tf_op jit(solution)/shard_map/psum | solution.py:45
  17.1 2.3 fusion.6
  21.5 26.8 %all-gather.7.cloned.1.call-done = bf16[384,4096]{1,0:T(8,128)(2,1)} async-done(((bf16[384,1024]{1,0:T(8,128)(2,1)}), bf16[384,4096]{1,0:T(8,128)(2,1)}) %all-gather.7.cloned.1.call-update) | async-done | bytes 3145744 | tf_op jit(solution)/shard_map/all_gather | solution.py:49
  48.3 151.2 %all-gather.11.cloned.1.call-done = bf16[2,4096,512]{2,1,0:T(8,128)(2,1)} async-done(((bf16[2,1024,512]{2,1,0:T(8,128)(2,1)}), bf16[2,4096,512]{2,1,0:T(8,128)(2,1)}) %all-gather.11.cloned.1.call-update) | async-done | bytes 8388624 | tf_op jit(solution)/shard_map/all_gather | solution.py:35
  199.5 5.0 fusion.23
  204.6 144.4 %all-gather.9.cloned.1.call-done = bf16[2,4096,512]{2,1,0:T(8,128)(2,1)} async-done(((bf16[2,1024,512]{2,1,0:T(8,128)(2,1)}), bf16[2,4096,512]{2,1,0:T(8,128)(2,1)}) %all-gather.9.cloned.1.call-update) | async-done | bytes 8388624 | tf_op jit(solution)/shard_map/all_gather | solution.py:34
  349.0 4.9 fusion.25
  355.2 143.0 %all-gather.15.cloned.1.call-done = bf16[8,512,1024]{2,1,0:T(8,128)(2,1)} async-done(((bf16[2,512,1024]{2,1,0:T(8,128)(2,1)}), bf16[8,512,1024]{2,1,0:T(8,128)(2,1)}) %all-gather.15.cloned.1.call-update) | async-done | bytes 8388624 | tf_op jit(solution)/shard_map/all_gather | solution.py:39
  498.2 5.9 fusion.62
  504.1 6.2 copy.35
  514.5 6.8 %all-reduce.1 = (f32[384]{0:T(512)S(1)}, f32[384]{0:T(512)S(1)}) all-reduce(f32[384]{0:T(512)S(1)} %get-tuple-element.25, f32[384]{0:T(512)S(1)} %get-tuple-element.26), channel_id=1, replica_groups=mesh['grp'=2,'sp'=4,'tp'=4] {'tp'}, use_global_device_ids=true, to_apply=%region_5.0 | all-reduce | flops 768 | bytes 6144 | tf_op jit(solution)/shard_map/psum | solution.py:57
  521.3 5.8 convolution_convert_fusion.1
  527.3 35.1 %reduce-scatter.3.cloned.1.call-done = bf16[384,1024]{1,0:T(8,128)(2,1)} async-done(((bf16[384,4096]{1,0:T(8,128)(2,1)}), bf16[384,1024]{1,0:T(8,128)(2,1)}) %reduce-scatter.3.cloned.1.call-update) | async-done | bytes 786448 | tf_op jit(solution)/shard_map/reduce_scatter | solution.py:67
  563.8 5.8 psum.45
  569.6 2.3 fusion.10
  572.2 29.1 %all-gather.13.cloned.1.call-done = bf16[384,4096]{1,0:T(8,128)(2,1)} async-done(((bf16[384,1024]{1,0:T(8,128)(2,1)}), bf16[384,4096]{1,0:T(8,128)(2,1)}) %all-gather.13.cloned.1.call-update) | async-done | bytes 3145744 | tf_op jit(solution)/shard_map/all_gather | solution.py:49
  601.2 5.2 fusion.21
  606.4 4.0 fusion.24
  610.5 3.4 collective-permute-start.1
  613.9 6.2 copy.40
  624.1 5.9 all-reduce
  630.0 5.8 convolution_convert_fusion
  635.9 37.9 %reduce-scatter.5.cloned.1.call-done = bf16[384,1024]{1,0:T(8,128)(2,1)} async-done(((bf16[384,4096]{1,0:T(8,128)(2,1)}), bf16[384,1024]{1,0:T(8,128)(2,1)}) %reduce-scatter.5.cloned.1.call-update) | async-done | bytes 786448 | tf_op jit(solution)/shard_map/reduce_scatter | solution.py:67
  673.7 2.4 fusion.11
  (65 shorter events, 15.4 us)
Async XLA Ops:
  6.5 41.8 %all-gather.7.cloned.1.call-start = ((), (), s32[]{:S(2)}) async-start(), calls=%async_computation.2 | async-start | bytes 3932160 | tf_op jit(solution)/shard_map/all_gather | solution.py:49
  19.3 2.1 copy-start.2
  19.4 2.1 copy-start.3
  19.4 180.2 %all-gather.11.cloned.1.call-start = ((), (), s32[]{:S(2)}) async-start(), calls=%async_computation.4 | async-start | bytes 10485760 | tf_op jit(solution)/shard_map/all_gather | solution.py:35
  20.1 328.8 %all-gather.9.cloned.1.call-start = ((), (), s32[]{:S(2)}) async-start(), calls=%async_computation.3 | async-start | bytes 10485760 | tf_op jit(solution)/shard_map/all_gather | solution.py:34
  20.9 477.3 %all-gather.15.cloned.1.call-start = ((), (), s32[]{:S(2)}) async-start(), calls=%async_computation.8 | async-start | bytes 10485760 | tf_op jit(solution)/shard_map/all_gather | solution.py:39
  21.4 540.9 %reduce-scatter.3.cloned.1.call-start = ((), (), s32[]{:S(2)}) async-start(), calls=%async_computation.5 | async-start | bytes 3932160 | tf_op jit(solution)/shard_map/reduce_scatter | solution.py:67
  353.9 156.4 %collective-permute-start = (bf16[30,512]{1,0:T(8,128)(2,1)S(1)}, bf16[30,512]{1,0:T(8,128)(2,1)S(1)}, u32[]{:S(2)}, u32[]{:S(2)}) collective-permute-start(bf16[30,512]{1,0:T(8,128)(2,1)S(1)} %slice.74), channel_id=1, source_target_pairs={{0,4},{4,8},{8,12},{1,5},{5,9},{9,13},{2,6},{6,10},{10,14},{3,7},{... | collective-permute-start | bytes 92168 | tf_op jit(solution)/shard_map/ppermute | solution.py:14
  510.3 0.9 copy-start.5
  510.3 0.9 copy-start.6
  527.2 35.2 %copy-start = (bf16[384,1024]{1,0:T(8,128)(2,1)S(1)}, bf16[384,1024]{1,0:T(8,128)(2,1)}, u32[]{:S(2)}) copy-start(bf16[384,1024]{1,0:T(8,128)(2,1)} %param.8) | copy-start | bytes 2359300
  527.2 74.0 %all-gather.13.cloned.1.call-start = ((), (), s32[]{:S(2)}) async-start(), calls=%async_computation.6 | async-start | bytes 3932160 | tf_op jit(solution)/shard_map/all_gather | solution.py:49
  571.9 101.8 %reduce-scatter.5.cloned.1.call-start = ((), (), s32[]{:S(2)}) async-start(), calls=%async_computation.7 | async-start | bytes 3932160 | tf_op jit(solution)/shard_map/reduce_scatter | solution.py:67
  601.2 5.2 copy-start.4
  610.5 9.6 %collective-permute-start.1 = (bf16[30,512]{1,0:T(8,128)(2,1)S(1)}, bf16[30,512]{1,0:T(8,128)(2,1)S(1)}, u32[]{:S(2)}, u32[]{:S(2)}) collective-permute-start(bf16[30,512]{1,0:T(8,128)(2,1)S(1)} %slice.81), channel_id=1, source_target_pairs={{0,4},{4,8},{8,12},{1,5},{5,9},{9,13},{2,6},{6,10},{10,14},{3,7},{... | collective-permute-start | bytes 92168 | tf_op jit(solution)/shard_map/ppermute | solution.py:14
  635.8 37.9 %copy-start.1 = (bf16[384,1024]{1,0:T(8,128)(2,1)S(1)}, bf16[384,1024]{1,0:T(8,128)(2,1)}, u32[]{:S(2)}) copy-start(bf16[384,1024]{1,0:T(8,128)(2,1)} %reduce-scatter.3.cloned.1.call-done) | copy-start | bytes 2359300
Sparse Core Ops, SparseCore 0:
  19.5 28.8 all-gather.6
  49.9 149.6 all-gather.10
  201.1 147.7 all-gather.8
  350.4 147.7 all-gather.14
  527.3 34.9 reduce-scatter.2
  572.1 29.1 all-gather.12
  636.0 37.7 reduce-scatter.4
